TPU v7x, 32 devices: a whole 2x2x4 slice. The times are simulated.
32 devices in a mesh: fs: 8 (over z, y), tp: 4 (over x, core).
Axes of the slice: x: 2, y: 2, z: 4, core: 2. Of those that a mesh axis runs over, the one named last changes fastest.
Arguments:
- tokens: bfloat16 [640, 3072], P('tp'), may hold values from -6 to 6
- gain_first: float32 [3072], replicated, may hold values from 0.1 to 1.9
- gain_second: float32 [3072], replicated, may hold values from 0.1 to 1.9
- gate_first: float32 [3072, 8192], P('fs', 'tp'), may hold values from -0.109375 to 0.109375
- up_first: float32 [3072, 8192], P('fs', 'tp'), may hold values from -0.109375 to 0.109375
- down_first: float32 [8192, 3072], P('fs', 'tp'), may hold values from -0.09375 to 0.09375
- gate_second: float32 [3072, 8192], P('fs', 'tp'), may hold values from -0.109375 to 0.109375
- up_second: float32 [3072, 8192], P('fs', 'tp'), may hold values from -0.109375 to 0.109375
- down_second: float32 [8192, 3072], P('fs', 'tp'), may hold values from -0.09375 to 0.09375
Outputs:
- result_rows: bfloat16 [640, 3072], P('tp')
- serve_gate_first: bfloat16 [3072, 8192], P(None, 'fs')
- serve_up_first: bfloat16 [3072, 8192], P(None, 'fs')
- serve_down_first: bfloat16 [8192, 3072], P('fs')
- serve_gate_second: bfloat16 [3072, 8192], P(None, 'fs')
- serve_up_second: bfloat16 [3072, 8192], P(None, 'fs')
- serve_down_second: bfloat16 [8192, 3072], P('fs')
All inputs are finite; a program needn't handle non-finite values.
Results may differ from a plain program's by a relative error of at most 0.011.
Values may be sent and summed in bfloat16 or wider, within the bound.
A program may use at most 192 MiB of HBM per device.

v0:
```python
import jax
import jax.numpy as jnp
from jax import lax
from jax.sharding import PartitionSpec as P


def plain_norm(values):
    values = values.astype(jnp.float32)
    center = jnp.mean(values, axis=-1, keepdims=True)
    spread = jnp.mean(jnp.square(values - center), axis=-1, keepdims=True)
    return (values - center) * lax.rsqrt(spread + 1e-05)


def half_step(normed, scales, w_gate, w_rising, w_down):
    gate_part = jnp.dot(normed, w_gate, preferred_element_type=jnp.float32)
    rising = jnp.dot(normed, w_rising, preferred_element_type=jnp.float32)
    hidden = (jax.nn.silu(gate_part) * rising).astype(jnp.bfloat16)
    partial_value = jnp.dot(hidden, w_down, preferred_element_type=jnp.float32)
    block = lax.psum(partial_value, "fs")
    mixed = 1.6817928 * scales[None, :] * normed.astype(jnp.float32) + 0.5 * block
    return plain_norm(mixed).astype(jnp.bfloat16)


def on_device(
    tokens,
    gain_first,
    gain_second,
    gate_first,
    up_first,
    down_first,
    gate_second,
    up_second,
    down_second,
):
    row_count = gate_first.shape[0]
    offset = lax.axis_index("fs") * row_count

    def fold_gain(weight, scales):
        picked = lax.dynamic_slice_in_dim(scales, offset, row_count, 0)
        return (picked[:, None] * weight).astype(jnp.bfloat16)

    widened = (
        lax.all_gather(fold_gain(gate_first, gain_first), "tp", axis=1, tiled=True),
        lax.all_gather(fold_gain(up_first, gain_first), "tp", axis=1, tiled=True),
        lax.all_gather(fold_gain(gate_second, gain_second), "tp", axis=1, tiled=True),
        lax.all_gather(fold_gain(up_second, gain_second), "tp", axis=1, tiled=True),
        lax.all_gather(down_first.astype(jnp.bfloat16), "tp", axis=1, tiled=True),
        lax.all_gather(down_second.astype(jnp.bfloat16), "tp", axis=1, tiled=True),
    )
    regrouped = (
        lax.all_to_all(widened[0], "fs", split_axis=1, concat_axis=0, tiled=True),
        lax.all_to_all(widened[1], "fs", split_axis=1, concat_axis=0, tiled=True),
        lax.all_to_all(widened[2], "fs", split_axis=1, concat_axis=0, tiled=True),
        lax.all_to_all(widened[3], "fs", split_axis=1, concat_axis=0, tiled=True),
    )
    serve_gate_first, serve_up_first, serve_gate_second, serve_up_second = regrouped
    serve_down_first = widened[4]
    serve_down_second = widened[5]
    normed_zero = plain_norm(tokens).astype(jnp.bfloat16)
    normed_one = half_step(
        normed_zero, gain_first, serve_gate_first, serve_up_first, serve_down_first
    )
    result_rows = half_step(
        normed_one, gain_second, serve_gate_second, serve_up_second, serve_down_second
    )
    return (
        result_rows,
        serve_gate_first,
        serve_up_first,
        serve_down_first,
        serve_gate_second,
        serve_up_second,
        serve_down_second,
    )


def solution(mesh):
    placed = (
        P("tp", None),
        P(),
        P(),
        P("fs", "tp"),
        P("fs", "tp"),
        P("fs", "tp"),
        P("fs", "tp"),
        P("fs", "tp"),
        P("fs", "tp"),
    )
    return jax.shard_map(
        on_device,
        mesh=mesh,
        in_specs=placed,
        out_specs=(
            P("tp", None),
            P(None, "fs"),
            P(None, "fs"),
            P("fs", None),
            P(None, "fs"),
            P(None, "fs"),
            P("fs", None),
        ),
        check_vma=False,
    )
```

profile of v0, /device:TPU:0, one launch (start us, length us, event | category | flops | bytes accessed | tf_op | source)
XLA Modules:
  0.0 865.7 jit_solution(17595812001735718184)
XLA Ops:
  8.0 5.5 multiply_convert_fusion.3
  14.3 48.5 %all-gather.7.cloned.1.call-done = bf16[384,8192]{1,0:T(8,128)(2,1)} async-done(((bf16[384,2048]{1,0:T(8,128)(2,1)}), bf16[384,8192]{1,0:T(8,128)(2,1)}) %all-gather.7.cloned.1.call-update) | async-done | bytes 6291472 | tf_op jit(solution)/shard_map/all_gather | solution.py:43
  62.7 6.5 copy.31
  69.2 5.8 all-to-all-start
  75.2 4.7 multiply_convert_fusion.1
  79.9 31.4 %all-gather.9.cloned.1.call-done = bf16[384,8192]{1,0:T(8,128)(2,1)} async-done(((bf16[384,2048]{1,0:T(8,128)(2,1)}), bf16[384,8192]{1,0:T(8,128)(2,1)}) %all-gather.9.cloned.1.call-update) | async-done | bytes 6291472 | tf_op jit(solution)/shard_map/all_gather | solution.py:44
  111.3 6.5 copy.30
  117.8 95.9 %all-to-all-done = bf16[384,8,1024]{2,0,1:T(8,128)(2,1)} async-done(((bf16[384,8,1024]{2,0,1:T(8,128)(2,1)}), bf16[384,8,1024]{2,0,1:T(8,128)(2,1)}, u32[]{:S(2)}, u32[]{:S(2)}) %all-to-all-start) | async-done | bytes 6291488 | tf_op jit(solution)/shard_map/all_to_all | solution.py:51
  213.7 5.0 all-to-all-start.1
  220.1 6.5 copy.29
  226.6 129.8 %all-to-all-done.1 = bf16[384,8,1024]{2,0,1:T(8,128)(2,1)} async-done(((bf16[384,8,1024]{2,0,1:T(8,128)(2,1)}), bf16[384,8,1024]{2,0,1:T(8,128)(2,1)}, u32[]{:S(2)}, u32[]{:S(2)}) %all-to-all-start.1) | async-done | bytes 6291488 | tf_op jit(solution)/shard_map/all_to_all | solution.py:52
  356.4 4.8 all-to-all-start.2
  363.0 4.0 fusion.16
  367.1 8.9 %fusion.7 = f32[160,3072]{1,0:T(8,128)} fusion(bf16[1024,3072]{1,0:T(8,128)(2,1)} %all-gather.11.cloned.1.call-done, bf16[3072,1024]{1,0:T(8,128)(2,1)} %bitcast.3, f32[160,1024]{1,0:T(8,128)S(1)} %fusion.16, bf16[160,3072]{1,0:T(8,128)(2,1)S(1)} %copy-done, f32[160]{0:T(256)S(1)} %add_rsqrt_fusion.2, f32[160]{0:T(256)S(1)} %broadcast_multiply_fusion.4), kind=kOutput, calls=%fused_computation.25 | convolution fusion | flops 2016215040 | bytes 16188672 | tf_op jit(solution)/shard_map/dot_general | solution.py:18
  376.0 34.6 %all-gather.15.cloned.1.call-done = bf16[384,8192]{1,0:T(8,128)(2,1)} async-done(((bf16[384,2048]{1,0:T(8,128)(2,1)}), bf16[384,8192]{1,0:T(8,128)(2,1)}) %all-gather.15.cloned.1.call-update) | async-done | bytes 6291472 | tf_op jit(solution)/shard_map/all_gather | solution.py:46
  410.6 6.5 copy.28
  417.1 107.7 %all-to-all-done.2 = bf16[384,8,1024]{2,0,1:T(8,128)(2,1)} async-done(((bf16[384,8,1024]{2,0,1:T(8,128)(2,1)}), bf16[384,8,1024]{2,0,1:T(8,128)(2,1)}, u32[]{:S(2)}, u32[]{:S(2)}) %all-to-all-start.2) | async-done | bytes 6291488 | tf_op jit(solution)/shard_map/all_to_all | solution.py:53
  524.8 4.8 all-to-all-start.3
  529.7 3.3 convert_element_type.54
  533.2 138.3 %all-reduce.3.cloned.1.call-done = f32[160,3072]{1,0:T(8,128)} async-done(((f32[160,3072]{1,0:T(8,128)}), f32[160,3072]{1,0:T(8,128)}) %all-reduce.3.cloned.1.call-update) | async-done | bytes 1966096 | tf_op jit(solution)/shard_map/psum | solution.py:19
  671.5 2.3 fusion.10
  675.5 4.7 fusion.18
  680.1 36.9 %all-gather.17.cloned.1.call-done = bf16[1024,3072]{1,0:T(8,128)(2,1)} async-done(((bf16[1024,768]{1,0:T(8,128)(2,1)}), bf16[1024,3072]{1,0:T(8,128)(2,1)}) %all-gather.17.cloned.1.call-update) | async-done | bytes 6291472 | tf_op jit(solution)/shard_map/all_gather | solution.py:48
  717.1 8.2 fusion.6
  725.3 98.6 %all-reduce.5.cloned.1.call-done = f32[160,3072]{1,0:T(8,128)} async-done(((f32[160,3072]{1,0:T(8,128)}), f32[160,3072]{1,0:T(8,128)}) %all-reduce.5.cloned.1.call-update) | async-done | bytes 1966096 | tf_op jit(solution)/shard_map/psum | solution.py:19
  823.8 2.1 fusion.11
  828.0 6.4 copy.40
  834.4 6.3 copy.41
  840.7 2.7 copy.42
  843.4 6.4 copy.43
  849.8 6.3 copy.44
  856.2 2.7 copy.45
  (60 shorter events, 9.0 us)
Async XLA Ops:
  7.2 55.6 %all-gather.7.cloned.1.call-start = ((), (), s32[]{:S(2)}) async-start(), calls=%async_computation.4 | async-start | bytes 7864320 | tf_op jit(solution)/shard_map/all_gather | solution.py:43
  13.5 97.7 %all-gather.9.cloned.1.call-start = ((), (), s32[]{:S(2)}) async-start(), calls=%async_computation.5 | async-start | bytes 7864320 | tf_op jit(solution)/shard_map/all_gather | solution.py:44
  69.2 5.8 copy-start.6
  69.2 5.9 copy-start.3
  69.2 144.4 %all-to-all-start = ((bf16[384,8,1024]{2,0,1:T(8,128)(2,1)}), bf16[384,8,1024]{2,0,1:T(8,128)(2,1)}, u32[]{:S(2)}, u32[]{:S(2)}) async-start(bf16[384,8,1024]{2,0,1:T(8,128)(2,1)} %bitcast.38), calls=%async_computation | async-start | bytes 12582912 | tf_op jit(solution)/shard_map/all_to_all | solution.py:51
  75.0 145.1 %all-gather.13.cloned.1.call-start = ((), (), s32[]{:S(2)}) async-start(), calls=%async_computation.8 | async-start | bytes 7864320 | tf_op jit(solution)/shard_map/all_gather | solution.py:45
  213.7 5.1 copy-start.4
  213.7 142.7 %all-to-all-start.1 = ((bf16[384,8,1024]{2,0,1:T(8,128)(2,1)}), bf16[384,8,1024]{2,0,1:T(8,128)(2,1)}, u32[]{:S(2)}, u32[]{:S(2)}) async-start(bf16[384,8,1024]{2,0,1:T(8,128)(2,1)} %bitcast.39), calls=%async_computation.1 | async-start | bytes 12582912 | tf_op jit(solution)/shard_map/all_to_all | solution.py:52
  218.7 148.4 %all-gather.11.cloned.1.call-start = ((), (), s32[]{:S(2)}) async-start(), calls=%async_computation.6 | async-start | bytes 7864320 | tf_op jit(solution)/shard_map/all_gather | solution.py:47
  356.4 168.4 %all-to-all-start.2 = ((bf16[384,8,1024]{2,0,1:T(8,128)(2,1)}), bf16[384,8,1024]{2,0,1:T(8,128)(2,1)}, u32[]{:S(2)}, u32[]{:S(2)}) async-start(bf16[384,8,1024]{2,0,1:T(8,128)(2,1)} %bitcast.36), calls=%async_computation.2 | async-start | bytes 12582912 | tf_op jit(solution)/shard_map/all_to_all | solution.py:53
  361.2 1.2 copy-start
  361.2 49.4 %all-gather.15.cloned.1.call-start = ((), (), s32[]{:S(2)}) async-start(), calls=%async_computation.9 | async-start | bytes 7864320 | tf_op jit(solution)/shard_map/all_gather | solution.py:46
  361.8 309.7 %all-reduce.3.cloned.1.call-start = ((), (), s32[]{:S(2)}) async-start(), calls=%async_computation.7 | async-start | bytes 3932160 | tf_op jit(solution)/shard_map/psum | solution.py:19
  524.8 192.3 %all-to-all-start.3 = ((bf16[384,8,1024]{2,0,1:T(8,128)(2,1)}), bf16[384,8,1024]{2,0,1:T(8,128)(2,1)}, u32[]{:S(2)}, u32[]{:S(2)}) async-start(bf16[384,8,1024]{2,0,1:T(8,128)(2,1)} %bitcast.37), calls=%async_computation.3 | async-start | bytes 12582912 | tf_op jit(solution)/shard_map/all_to_all | solution.py:54
  529.6 3.6 copy-start.5
  529.6 187.4 %all-gather.17.cloned.1.call-start = ((), (), s32[]{:S(2)}) async-start(), calls=%async_computation.10 | async-start | bytes 7864320 | tf_op jit(solution)/shard_map/all_gather | solution.py:48
  533.0 290.8 %all-reduce.5.cloned.1.call-start = ((), (), s32[]{:S(2)}) async-start(), calls=%async_computation.11 | async-start | bytes 3932160 | tf_op jit(solution)/shard_map/psum | solution.py:19
  671.5 2.3 copy-start.1
  823.8 2.1 copy-start.2
  828.0 12.7 %slice-start = ((s8[6291456]{0:T(1024)(128)(4,1)}), s8[4194304]{0:T(1024)(128)(4,1)S(1)}, s32[]{:S(2)}) async-start(s8[6291456]{0:T(1024)(128)(4,1)} %bitcast.40), calls=%async_computation.12 | async-start | bytes 8388608
  834.4 6.4 slice-start.1
  843.4 12.7 %slice-start.2 = ((s8[6291456]{0:T(1024)(128)(4,1)}), s8[4194304]{0:T(1024)(128)(4,1)S(1)}, s32[]{:S(2)}) async-start(s8[6291456]{0:T(1024)(128)(4,1)} %bitcast.42), calls=%async_computation.14 | async-start | bytes 8388608
  849.8 6.4 slice-start.3
Sparse Core Ops, SparseCore 0:
  13.6 49.0 all-gather.6
  64.9 46.3 all-gather.8
  113.4 46.3 all-gather.12
  221.3 46.7 all-gather.10
  363.8 46.7 all-gather.14
  414.6 256.8 all-reduce.2
  673.6 43.3 all-gather.16
  725.4 98.3 all-reduce.4
where the time goes:
time: 866 us
  waiting for transfers between devices  723 us (83%)
  local copies, waits for them, and re-layouts  58.3 us (7%)
  matrix products  25.7 us (3%)
  other arithmetic  23.5 us (3%)
  starting transfers between devices  20.9 us (2%)
  between operations  14.3 us (2%)
    psum x2, waiting for transfers between devices, half_step(): block = lax.psum(partial_value, 'fs')  237 us
    all_to_all x1, waiting for transfers between devices, on_device(): lax.all_to_all(widened[1], 'fs', split_axis=1, concat_axis=0, tiled=True)  130 us
    all_to_all x1, waiting for transfers between devices, on_device(): lax.all_to_all(widened[2], 'fs', split_axis=1, concat_axis=0, tiled=True)  108 us
    all_to_all x1, waiting for transfers between devices, on_device(): lax.all_to_all(widened[0], 'fs', split_axis=1, concat_axis=0, tiled=True)  95.9 us
    all_gather x1, waiting for transfers between devices, on_device(): lax.all_gather(fold_gain(gate_first, gain_first), 'tp', axis=1, tiled=True)  48.5 us
    all_gather x1, waiting for transfers between devices, on_device(): lax.all_gather(down_second.astype(jnp.bfloat16), 'tp', axis=1, tiled=True)  36.9 us
    all_gather x1, waiting for transfers between devices, on_device(): lax.all_gather(fold_gain(up_second, gain_second), 'tp', axis=1, tiled=True)  34.6 us
    unnamed x28, local copies, waits for them, and re-layouts  31.5 us
  transfers between devices with their start and end apart: 12, of which 9 were waited for; matrix products, arithmetic and copies ran while one was open for 7% of the time, Pallas kernels for 0%

commit v1 on v0

--- a/solution.py
+++ b/solution.py
@@ -16,7 +16,10 @@
     rising = jnp.dot(normed, w_rising, preferred_element_type=jnp.float32)
     hidden = (jax.nn.silu(gate_part) * rising).astype(jnp.bfloat16)
     partial_value = jnp.dot(hidden, w_down, preferred_element_type=jnp.float32)
-    block = lax.psum(partial_value, "fs")
+    size, block = (lax.axis_size("fs"), partial_value)
+    for stride in [1 << k for k in range(size.bit_length() - 1)]:
+        swap = [(i, i ^ stride) for i in range(size)]
+        block = block + lax.ppermute(block, "fs", swap)
     mixed = 1.6817928 * scales[None, :] * normed.astype(jnp.float32) + 0.5 * block
     return plain_norm(mixed).astype(jnp.bfloat16)
 

time: 866 us -> 1000 us (1.15)
  waiting for transfers between devices: 723 us -> 858 us
    ppermute x0 -> x6, waiting for transfers between devices: none -> 421 us  [half_step(): block = block + lax.ppermute(block, 'fs', swap)]
    psum x2 -> x0, waiting for transfers between devices: 237 us -> none  [half_step(): block = lax.psum(partial_value, 'fs')]
    all_gather x1, waiting for transfers between devices: 36.9 us -> 0.02 us  [on_device(): lax.all_gather(down_second.astype(jnp.bfloat16), 'tp', axis=1, tiled=True)]
    all_gather x1, waiting for transfers between devices: 34.6 us -> 0.02 us  [on_device(): lax.all_gather(fold_gain(up_second, gain_second), 'tp', axis=1, tiled=True)]
    all_to_all x1, waiting for transfers between devices: 108 us -> 129 us  [on_device(): lax.all_to_all(widened[2], 'fs', split_axis=1, concat_axis=0, tiled=True)]
    unnamed x28 -> x26, local copies, waits for them, and re-layouts: 31.5 us -> 32.1 us
  transfers between devices with their start and end apart: 12 -> 16, of which waited for: 9 -> 11; matrix products, arithmetic and copies ran while one was open for 7% -> 5% of each run, Pallas kernels for 0% -> 0%
where the time goes in v1:
time: 1000 us
  waiting for transfers between devices  858 us (86%)
  local copies, waits for them, and re-layouts  58.9 us (6%)
  matrix products  26.2 us (3%)
  starting transfers between devices  23.9 us (2%)
  other arithmetic  19.2 us (2%)
  between operations  14.3 us (1%)
    ppermute x6, waiting for transfers between devices, half_step(): block = block + lax.ppermute(block, 'fs', swap)  421 us
    all_to_all x1, waiting for transfers between devices, on_device(): lax.all_to_all(widened[1], 'fs', split_axis=1, concat_axis=0, tiled=True)  131 us
    all_to_all x1, waiting for transfers between devices, on_device(): lax.all_to_all(widened[2], 'fs', split_axis=1, concat_axis=0, tiled=True)  129 us
    all_to_all x1, waiting for transfers between devices, on_device(): lax.all_to_all(widened[0], 'fs', split_axis=1, concat_axis=0, tiled=True)  95.9 us
    all_gather x1, waiting for transfers between devices, on_device(): lax.all_gather(fold_gain(gate_first, gain_first), 'tp', axis=1, tiled=True)  48.5 us
    unnamed x26, local copies, waits for them, and re-layouts  32.1 us
    all_gather x1, waiting for transfers between devices, on_device(): lax.all_gather(fold_gain(up_first, gain_first), 'tp', axis=1, tiled=True)  31.4 us
  transfers between devices with their start and end apart: 16, of which 11 were waited for; matrix products, arithmetic and copies ran while one was open for 5% of the time, Pallas kernels for 0%

profile of v1, /device:TPU:0, one launch (start us, length us, event | category | flops | bytes accessed | tf_op | source)
XLA Modules:
  0.0 1000.9 jit_solution(2677460739637218908)
XLA Ops:
  8.0 5.5 multiply_convert_fusion.3
  14.3 48.5 %all-gather.7.cloned.1.call-done = bf16[384,8192]{1,0:T(8,128)(2,1)} async-done(((bf16[384,2048]{1,0:T(8,128)(2,1)}), bf16[384,8192]{1,0:T(8,128)(2,1)}) %all-gather.7.cloned.1.call-update) | async-done | bytes 6291472 | tf_op jit(solution)/shard_map/all_gather | solution.py:46
  62.7 6.5 copy.31
  69.2 5.8 all-to-all-start
  75.2 4.7 multiply_convert_fusion
  79.9 31.4 %all-gather.9.cloned.1.call-done = bf16[384,8192]{1,0:T(8,128)(2,1)} async-done(((bf16[384,2048]{1,0:T(8,128)(2,1)}), bf16[384,8192]{1,0:T(8,128)(2,1)}) %all-gather.9.cloned.1.call-update) | async-done | bytes 6291472 | tf_op jit(solution)/shard_map/all_gather | solution.py:47
  111.3 6.5 copy.30
  117.8 95.9 %all-to-all-done = bf16[384,8,1024]{2,0,1:T(8,128)(2,1)} async-done(((bf16[384,8,1024]{2,0,1:T(8,128)(2,1)}), bf16[384,8,1024]{2,0,1:T(8,128)(2,1)}, u32[]{:S(2)}, u32[]{:S(2)}) %all-to-all-start) | async-done | bytes 6291488 | tf_op jit(solution)/shard_map/all_to_all | solution.py:54
  213.7 4.8 all-to-all-start.1
  219.0 6.5 copy.29
  225.5 130.6 %all-to-all-done.1 = bf16[384,8,1024]{2,0,1:T(8,128)(2,1)} async-done(((bf16[384,8,1024]{2,0,1:T(8,128)(2,1)}), bf16[384,8,1024]{2,0,1:T(8,128)(2,1)}, u32[]{:S(2)}, u32[]{:S(2)}) %all-to-all-start.1) | async-done | bytes 6291488 | tf_op jit(solution)/shard_map/all_to_all | solution.py:55
  356.1 5.0 all-to-all-start.2
  362.6 6.5 copy.28
  369.1 129.3 %all-to-all-done.2 = bf16[384,8,1024]{2,0,1:T(8,128)(2,1)} async-done(((bf16[384,8,1024]{2,0,1:T(8,128)(2,1)}), bf16[384,8,1024]{2,0,1:T(8,128)(2,1)}, u32[]{:S(2)}, u32[]{:S(2)}) %all-to-all-start.2) | async-done | bytes 6291488 | tf_op jit(solution)/shard_map/all_to_all | solution.py:56
  498.4 5.0 all-to-all-start.3
  506.8 4.9 fusion.15
  511.7 9.0 fusion.5
  522.5 92.0 %collective-permute-done = f32[160,3072]{1,0:T(8,128)S(1)} collective-permute-done((f32[160,3072]{1,0:T(8,128)S(1)}, f32[160,3072]{1,0:T(8,128)S(1)}, u32[]{:S(2)}, u32[]{:S(2)}) %collective-permute-start) | collective-permute-done | bytes 1966112 | tf_op jit(solution)/shard_map/ppermute | solution.py:22
  614.9 67.9 %collective-permute-done.1 = f32[160,3072]{1,0:T(8,128)S(1)} collective-permute-done((f32[160,3072]{1,0:T(8,128)S(1)}, f32[160,3072]{1,0:T(8,128)S(1)}, u32[]{:S(2)}, u32[]{:S(2)}) %collective-permute-start.1) | collective-permute-done | bytes 1966112 | tf_op jit(solution)/shard_map/ppermute | solution.py:22
  683.5 87.0 %collective-permute-done.2 = f32[160,3072]{1,0:T(8,128)S(1)} collective-permute-done((f32[160,3072]{1,0:T(8,128)S(1)}, f32[160,3072]{1,0:T(8,128)S(1)}, u32[]{:S(2)}, u32[]{:S(2)}) %collective-permute-start.2) | collective-permute-done | bytes 1966112 | tf_op jit(solution)/shard_map/ppermute | solution.py:22
  771.6 4.0 fusion.19
  775.7 8.3 fusion.6
  783.9 45.0 %collective-permute-done.3 = f32[160,3072]{1,0:T(8,128)S(1)} collective-permute-done((f32[160,3072]{1,0:T(8,128)}, f32[160,3072]{1,0:T(8,128)S(1)}, u32[]{:S(2)}, u32[]{:S(2)}) %collective-permute-start.3) | collective-permute-done | bytes 1966112 | tf_op jit(solution)/shard_map/ppermute | solution.py:22
  828.9 1.8 add.70
  830.8 43.9 %collective-permute-done.4 = f32[160,3072]{1,0:T(8,128)S(1)} collective-permute-done((f32[160,3072]{1,0:T(8,128)S(1)}, f32[160,3072]{1,0:T(8,128)S(1)}, u32[]{:S(2)}, u32[]{:S(2)}) %collective-permute-start.4) | collective-permute-done | bytes 1966112 | tf_op jit(solution)/shard_map/ppermute | solution.py:22
  875.4 85.6 %collective-permute-done.5 = f32[160,3072]{1,0:T(8,128)S(1)} collective-permute-done((f32[160,3072]{1,0:T(8,128)S(1)}, f32[160,3072]{1,0:T(8,128)S(1)}, u32[]{:S(2)}, u32[]{:S(2)}) %collective-permute-start.5) | collective-permute-done | bytes 1966112 | tf_op jit(solution)/shard_map/ppermute | solution.py:22
  963.2 6.4 copy.38
  969.6 6.3 copy.39
  976.0 2.7 copy.40
  978.7 6.4 copy.41
  985.0 6.3 copy.42
  991.4 2.7 copy.43
  (67 shorter events, 14.0 us)
Async XLA Ops:
  7.2 55.6 %all-gather.7.cloned.1.call-start = ((), (), s32[]{:S(2)}) async-start(), calls=%async_computation.4 | async-start | bytes 7864320 | tf_op jit(solution)/shard_map/all_gather | solution.py:46
  13.5 97.7 %all-gather.9.cloned.1.call-start = ((), (), s32[]{:S(2)}) async-start(), calls=%async_computation.5 | async-start | bytes 7864320 | tf_op jit(solution)/shard_map/all_gather | solution.py:47
  69.2 5.8 copy-start.5
  69.2 5.9 copy-start.1
  69.2 144.4 %all-to-all-start = ((bf16[384,8,1024]{2,0,1:T(8,128)(2,1)}), bf16[384,8,1024]{2,0,1:T(8,128)(2,1)}, u32[]{:S(2)}, u32[]{:S(2)}) async-start(bf16[384,8,1024]{2,0,1:T(8,128)(2,1)} %bitcast.39), calls=%async_computation | async-start | bytes 12582912 | tf_op jit(solution)/shard_map/all_to_all | solution.py:54
  75.0 144.0 %all-gather.13.cloned.1.call-start = ((), (), s32[]{:S(2)}) async-start(), calls=%async_computation.7 | async-start | bytes 7864320 | tf_op jit(solution)/shard_map/all_gather | solution.py:48
  213.7 142.5 %all-to-all-start.1 = ((bf16[384,8,1024]{2,0,1:T(8,128)(2,1)}), bf16[384,8,1024]{2,0,1:T(8,128)(2,1)}, u32[]{:S(2)}, u32[]{:S(2)}) async-start(bf16[384,8,1024]{2,0,1:T(8,128)(2,1)} %bitcast.40), calls=%async_computation.1 | async-start | bytes 12582912 | tf_op jit(solution)/shard_map/all_to_all | solution.py:55
  218.4 144.2 %all-gather.15.cloned.1.call-start = ((), (), s32[]{:S(2)}) async-start(), calls=%async_computation.8 | async-start | bytes 7864320 | tf_op jit(solution)/shard_map/all_gather | solution.py:49
  356.1 5.1 copy-start.2
  356.1 142.3 %all-to-all-start.2 = ((bf16[384,8,1024]{2,0,1:T(8,128)(2,1)}), bf16[384,8,1024]{2,0,1:T(8,128)(2,1)}, u32[]{:S(2)}, u32[]{:S(2)}) async-start(bf16[384,8,1024]{2,0,1:T(8,128)(2,1)} %bitcast.41), calls=%async_computation.2 | async-start | bytes 12582912 | tf_op jit(solution)/shard_map/all_to_all | solution.py:56
  361.2 150.5 %all-gather.11.cloned.1.call-start = ((), (), s32[]{:S(2)}) async-start(), calls=%async_computation.6 | async-start | bytes 7864320 | tf_op jit(solution)/shard_map/all_gather | solution.py:50
  498.4 5.3 copy-start.3
  498.4 277.3 %all-to-all-start.3 = ((bf16[384,8,1024]{2,0,1:T(8,128)(2,1)}), bf16[384,8,1024]{2,0,1:T(8,128)(2,1)}, u32[]{:S(2)}, u32[]{:S(2)}) async-start(bf16[384,8,1024]{2,0,1:T(8,128)(2,1)} %bitcast.38), calls=%async_computation.3 | async-start | bytes 12582912 | tf_op jit(solution)/shard_map/all_to_all | solution.py:57
  503.4 272.2 %all-gather.17.cloned.1.call-start = ((), (), s32[]{:S(2)}) async-start(), calls=%async_computation.9 | async-start | bytes 7864320 | tf_op jit(solution)/shard_map/all_gather | solution.py:51
  505.0 1.2 copy-start
  520.8 93.8 %collective-permute-start = (f32[160,3072]{1,0:T(8,128)S(1)}, f32[160,3072]{1,0:T(8,128)S(1)}, u32[]{:S(2)}, u32[]{:S(2)}) collective-permute-start(f32[160,3072]{1,0:T(8,128)S(1)} %fusion.5), channel_id=1, source_target_pairs={{0,4},{4,0},{8,12},{12,8},{16,20},{20,16},{24,28},{28,24},{1,5},{5... | collective-permute-start | bytes 5898248 | tf_op jit(solution)/shard_map/ppermute | solution.py:22
  614.8 68.8 %copy-start.4 = (f32[3072]{0:T(1024)S(1)}, f32[3072]{0:T(1024)}, u32[]{:S(2)}) copy-start(f32[3072]{0:T(1024)} %param.10) | copy-start | bytes 36868
  614.8 68.0 %collective-permute-start.1 = (f32[160,3072]{1,0:T(8,128)S(1)}, f32[160,3072]{1,0:T(8,128)S(1)}, u32[]{:S(2)}, u32[]{:S(2)}) collective-permute-start(f32[160,3072]{1,0:T(8,128)S(1)} %add.64), channel_id=1, source_target_pairs={{0,8},{4,12},{8,0},{12,4},{16,24},{20,28},{24,16},{28,20},{1,9},{5... | collective-permute-start | bytes 5898248 | tf_op jit(solution)/shard_map/ppermute | solution.py:22
  683.0 87.6 %collective-permute-start.2 = (f32[160,3072]{1,0:T(8,128)S(1)}, f32[160,3072]{1,0:T(8,128)S(1)}, u32[]{:S(2)}, u32[]{:S(2)}) collective-permute-start(f32[160,3072]{1,0:T(8,128)S(1)} %add.65), channel_id=1, source_target_pairs={{0,16},{4,20},{8,24},{12,28},{16,0},{20,4},{24,8},{28,12},{1,17},{... | collective-permute-start | bytes 5898248 | tf_op jit(solution)/shard_map/ppermute | solution.py:22
  783.9 45.0 %collective-permute-start.3 = (f32[160,3072]{1,0:T(8,128)}, f32[160,3072]{1,0:T(8,128)S(1)}, u32[]{:S(2)}, u32[]{:S(2)}) collective-permute-start(f32[160,3072]{1,0:T(8,128)} %fusion.6), channel_id=1, source_target_pairs={{0,4},{4,0},{8,12},{12,8},{16,20},{20,16},{24,28},{28,24},{1,5},{5... | collective-permute-start | bytes 5898248 | tf_op jit(solution)/shard_map/ppermute | solution.py:22
  830.7 44.0 %collective-permute-start.4 = (f32[160,3072]{1,0:T(8,128)S(1)}, f32[160,3072]{1,0:T(8,128)S(1)}, u32[]{:S(2)}, u32[]{:S(2)}) collective-permute-start(f32[160,3072]{1,0:T(8,128)S(1)} %add.70), channel_id=1, source_target_pairs={{0,8},{4,12},{8,0},{12,4},{16,24},{20,28},{24,16},{28,20},{1,9},{5... | collective-permute-start | bytes 5898248 | tf_op jit(solution)/shard_map/ppermute | solution.py:22
  874.9 86.1 %collective-permute-start.5 = (f32[160,3072]{1,0:T(8,128)S(1)}, f32[160,3072]{1,0:T(8,128)S(1)}, u32[]{:S(2)}, u32[]{:S(2)}) collective-permute-start(f32[160,3072]{1,0:T(8,128)S(1)} %add.71), channel_id=1, source_target_pairs={{0,16},{4,20},{8,24},{12,28},{16,0},{20,4},{24,8},{28,12},{1,17},{... | collective-permute-start | bytes 5898248 | tf_op jit(solution)/shard_map/ppermute | solution.py:22
  963.2 12.7 %slice-start.2 = ((s8[6291456]{0:T(1024)(128)(4,1)}), s8[4194304]{0:T(1024)(128)(4,1)S(1)}, s32[]{:S(2)}) async-start(s8[6291456]{0:T(1024)(128)(4,1)} %bitcast.42), calls=%async_computation.12 | async-start | bytes 8388608
  969.6 6.4 slice-start.3
  978.7 12.7 %slice-start = ((s8[6291456]{0:T(1024)(128)(4,1)}), s8[4194304]{0:T(1024)(128)(4,1)S(1)}, s32[]{:S(2)}) async-start(s8[6291456]{0:T(1024)(128)(4,1)} %bitcast.36), calls=%async_computation.10 | async-start | bytes 8388608
  985.0 6.4 slice-start.1
Sparse Core Ops, SparseCore 0:
  13.6 49.0 all-gather.6
  64.9 46.3 all-gather.8
  113.4 46.3 all-gather.12
  221.1 46.7 all-gather.14
  363.8 46.7 all-gather.10
  506.1 46.7 all-gather.16
